TPU v7x, 32 devices: a whole 2x2x4 slice. The times are simulated.
32 devices in a mesh: sp: 8 (over z, x), tp: 4 (over y, core).
Axes of the slice: x: 2, y: 2, z: 4, core: 2. Of those that a mesh axis runs over, the one named last changes fastest.
Arguments:
- stream: bfloat16 [1024, 2048], P(('sp', 'tp')), may hold values from -2.5 to 2.5
- recurrence_input: bfloat16 [1024, 2, 1024], P('sp', None, 'tp'), may hold values from -6 to 6
- output_gate_input: bfloat16 [1024, 2, 1024], P('sp', None, 'tp'), may hold values from -6 to 6
- convolution_taps: bfloat16 [4, 2, 1024], P(None, None, 'tp'), may hold values from -4 to 4
- first_group_gates: bfloat16 [2, 16, 64, 64], P(None, 'tp'), may hold values from -0.75 to 0.75
- second_group_gates: bfloat16 [2, 8, 128, 128], P(None, 'tp'), may hold values from -0.5 to 0.5
- channel_decay: float32 [2, 1024], P(None, 'tp'), may hold values from 4.7 to 13.6
- position_log_extra: float32 [1024, 2, 1024], P('sp', None, 'tp'), may hold values from -1.4 to 0, as said below
- recurrence_output_weight: bfloat16 [2, 1024, 2048], P(None, 'tp'), may hold values from -0.125 to 0.125
- first_norm_gain: float32 [2048], replicated, may hold values from 0.1 to 1.9
- first_norm_bias: float32 [2048], replicated, may hold values from -1.75 to 1.75
- routed_expert_index: int32 [1024, 4], P('sp'), may hold values from 0 to 7, all different within a row; in each aligned block of 32 rows (0 to 31, 32 to 63, ...) at most 20 rows name the same one
- routed_expert_weight: float32 [1024, 4], P('sp'), may hold values from 0.25 to 1
- routed_gate_weight: bfloat16 [8, 2048, 512], P('sp', None, 'tp'), may hold values from -0.125 to 0.125
- routed_up_weight: bfloat16 [8, 2048, 512], P('sp', None, 'tp'), may hold values from -0.125 to 0.125
- routed_down_weight: bfloat16 [8, 512, 2048], P('sp', 'tp'), may hold values from -0.25 to 0.25
- shared_gate_weight: bfloat16 [2048, 512], replicated, may hold values from -0.125 to 0.125
- shared_up_weight: bfloat16 [2048, 512], replicated, may hold values from -0.125 to 0.125
- shared_down_weight: bfloat16 [512, 2048], replicated, may hold values from -0.25 to 0.25
- second_norm_gain: float32 [2048], replicated, may hold values from 0.1 to 1.9
- second_norm_bias: float32 [2048], replicated, may hold values from -1.75 to 1.75
Outputs:
- result: bfloat16 [1024, 2048], P(('sp', 'tp'))
Inputs may be any that keep to these rules, and one draw needn't show every extreme that they name: `routed_expert_index`: each row names 4 different experts. In each aligned block of 32 rows no expert is named more than 20 times, and in some block an expert is named exactly 20 times. `position_log_extra`: every entry is negative.
All inputs are finite; a program needn't handle non-finite values.
Results may differ from a plain program's by a relative error of at most 0.015.
Values may be sent and summed in bfloat16 or wider, within the bound.
A program may use at most 64 MiB of HBM per device.

v0:
```python
import jax
import jax.numpy as jnp
from jax import lax
from jax.sharding import PartitionSpec as P

RESIDUAL_SCALE = 8.0**0.25
NORM_EPSILON = 1e-05


def entering(part, axis, combine, identity):
    place = lax.axis_index(axis)
    gathered = jax.tree.map(lambda a: lax.all_gather(a, axis), part)
    state = jax.tree.map(lambda a, e: jnp.zeros_like(a) + jnp.asarray(e, a.dtype), part, identity)

    def one(step, state):
        return combine(
            state, jax.tree.map(lambda a: lax.dynamic_index_in_dim(a, step, 0, False), gathered)
        )

    return lax.fori_loop(0, place, one, state)


def shifted(shard, axis, by):
    count = lax.axis_size(axis)
    pairs = [(i, i + by) for i in range(count) if 0 <= i + by < count]
    return lax.ppermute(shard, axis, pairs)


def layer_norm(values, gain_vec, bias_vec):
    row_mean = jnp.mean(values, axis=-1, keepdims=True)
    spread = jnp.mean(jnp.square(values - row_mean), axis=-1, keepdims=True)
    return (values - row_mean) * lax.rsqrt(spread + NORM_EPSILON) * gain_vec + bias_vec


def block_gates(conv_rows, weights, head_size):
    length = conv_rows.shape[0]
    head_rows = conv_rows.reshape(length, -1, head_size)
    pre_act = jnp.einsum("thc,ghcd->gthd", head_rows, weights, preferred_element_type=jnp.float32)
    gate_pair = jax.nn.sigmoid(pre_act).reshape(2, length, -1)
    return (gate_pair[0], gate_pair[1])


def chain_link(first_part, second_part):
    return (first_part[0] * second_part[0], second_part[0] * first_part[1] + second_part[1])


def carried(totals):
    unity = jnp.ones_like(totals[0])
    nought = jnp.zeros_like(totals[1])
    return entering(totals, "sp", chain_link, (unity, nought))[1]


def expert_terms(picked, letters, gate_w, up_w, down_w):
    gate_form = letters + "d,ldf->" + letters + "f"
    down_form = letters + "f,lfd->" + letters + "d"
    gated = jnp.einsum(gate_form, picked, gate_w, preferred_element_type=jnp.float32)
    lifted = jnp.einsum(gate_form, picked, up_w, preferred_element_type=jnp.float32)
    hidden = (jax.nn.silu(gated) * lifted).astype(jnp.bfloat16)
    return jnp.einsum(down_form, hidden, down_w, preferred_element_type=jnp.float32)


def shards(
    stream,
    recurrence_input,
    output_gate_input,
    convolution_taps,
    first_group_gates,
    second_group_gates,
    channel_decay,
    position_log_extra,
    recurrence_output_weight,
    first_norm_gain,
    first_norm_bias,
    routed_expert_index,
    routed_expert_weight,
    routed_gate_weight,
    routed_up_weight,
    routed_down_weight,
    shared_gate_weight,
    shared_up_weight,
    shared_down_weight,
    second_norm_gain,
    second_norm_bias,
):
    length = recurrence_input.shape[0]
    tap_count = convolution_taps.shape[0]
    border = shifted(recurrence_input[length - (tap_count - 1) :], "sp", 1)
    padded = jnp.concatenate([border, recurrence_input], axis=0).astype(jnp.float32)
    tap_weights = convolution_taps.astype(jnp.float32)
    summed = tap_weights[0] * padded[0:length]
    for offset in range(1, tap_count):
        summed = summed + tap_weights[offset] * padded[offset : offset + length]
    conv_rows = summed.astype(jnp.bfloat16)
    recur_a, input_a = block_gates(conv_rows[:, 0], first_group_gates, first_group_gates.shape[-1])
    recur_b, input_b = block_gates(
        conv_rows[:, 1], second_group_gates, second_group_gates.shape[-1]
    )
    recurrence_gate = jnp.stack([recur_a, recur_b], axis=1)
    input_gate = jnp.stack([input_a, input_b], axis=1)
    decay_logarithm = -8.0 * recurrence_gate * jax.nn.softplus(-channel_decay) + position_log_extra
    decay_rate = jnp.exp(decay_logarithm)
    driving = (
        jnp.sqrt(-jnp.expm1(2.0 * decay_logarithm)) * input_gate * conv_rows.astype(jnp.float32)
    )
    running = jnp.cumsum(decay_logarithm, axis=0)
    tail_sum = jnp.sum(jnp.exp(running[-1] - running) * driving, axis=0)
    incoming = carried((jnp.exp(running[-1]), tail_sum))
    opening = driving[:1] + decay_rate[:1] * incoming
    started = jnp.concatenate([opening, driving[1:]], axis=0)
    states = lax.associative_scan(chain_link, (decay_rate, started), axis=0)[1]
    branch_output = (jax.nn.gelu(output_gate_input.astype(jnp.float32)) * states).astype(
        jnp.bfloat16
    )
    tp_count = lax.axis_size("tp")
    quarter = length // tp_count
    mixed = lax.psum_scatter(
        jnp.einsum(
            "tgc,gcd->td",
            branch_output,
            recurrence_output_weight,
            preferred_element_type=jnp.float32,
        ).astype(jnp.bfloat16),
        "tp",
        scatter_dimension=0,
        tiled=True,
    ).astype(jnp.float32)
    normed = layer_norm(
        RESIDUAL_SCALE * stream.astype(jnp.float32) + mixed, first_norm_gain, first_norm_bias
    ).astype(jnp.bfloat16)
    width = normed.shape[1]
    top_count = routed_expert_index.shape[1]
    local_count = routed_gate_weight.shape[0]
    expert_count = local_count * lax.axis_size("sp")
    capacity = max(2, 5 * quarter * top_count // (4 * expert_count))
    block_ids = routed_expert_index.reshape(tp_count, quarter * top_count)
    onehot = (
        block_ids[:, :, None] == jnp.arange(expert_count, dtype=jnp.int32)[None, None, :]
    ).astype(jnp.int32)
    slot_ranks = jnp.sum((jnp.cumsum(onehot, axis=1) - onehot) * onehot, axis=2)
    own_index = lax.axis_index("tp")
    own_ids = lax.dynamic_index_in_dim(block_ids, own_index, 0, keepdims=False)
    own_ranks = lax.dynamic_index_in_dim(slot_ranks, own_index, 0, keepdims=False)
    blank_row = jnp.zeros((1, width), jnp.bfloat16)
    gathered = lax.all_gather(normed, "tp", axis=0, tiled=True)
    padded_rows = jnp.concatenate([gathered, blank_row], axis=0)
    block_index = jnp.arange(tp_count, dtype=jnp.int32)[:, None]
    targets = (block_ids * tp_count + block_index) * capacity + slot_ranks
    sources = (
        jnp.arange(length * top_count, dtype=jnp.int32).reshape(tp_count, quarter * top_count)
        // top_count
    )
    table = jnp.full((expert_count * tp_count * capacity,), length, jnp.int32)
    table = table.at[targets.reshape(-1)].set(sources.reshape(-1))
    outgoing = jnp.take(padded_rows, table, axis=0).reshape(expert_count, tp_count, capacity, width)
    arrived = lax.all_to_all(outgoing, "sp", split_axis=0, concat_axis=0, tiled=True)
    slots = arrived.shape[2]
    shaped = arrived.reshape(-1, local_count, tp_count, slots, width)
    partial_value = expert_terms(
        shaped, "slxc", routed_gate_weight, routed_up_weight, routed_down_weight
    )
    summed_rows = lax.psum_scatter(
        partial_value.astype(jnp.bfloat16), "tp", scatter_dimension=2, tiled=True
    )
    leaving = summed_rows.reshape(-1, 1, slots, width)
    returned = lax.all_to_all(leaving, "sp", split_axis=0, concat_axis=0, tiled=True)
    picked_rows = returned.reshape(expert_count * capacity, width)[own_ids * capacity + own_ranks]
    own_weights = lax.dynamic_slice_in_dim(routed_expert_weight, own_index * quarter, quarter, 0)
    routed = jnp.sum(
        own_weights[:, :, None]
        * picked_rows.reshape(quarter, top_count, width).astype(jnp.float32),
        axis=1,
    )
    shared_hidden = (
        jax.nn.silu(jnp.dot(normed, shared_gate_weight, preferred_element_type=jnp.float32))
        * jnp.dot(normed, shared_up_weight, preferred_element_type=jnp.float32)
    ).astype(jnp.bfloat16)
    shared_out = jnp.dot(shared_hidden, shared_down_weight, preferred_element_type=jnp.float32)
    final = layer_norm(
        RESIDUAL_SCALE * normed.astype(jnp.float32) + (shared_out + routed),
        second_norm_gain,
        second_norm_bias,
    )
    return final.astype(jnp.bfloat16)


def solution(mesh):
    in_specs = (
        P(("sp", "tp"), None),
        P("sp", None, "tp"),
        P("sp", None, "tp"),
        P(None, None, "tp"),
        P(None, "tp", None, None),
        P(None, "tp", None, None),
        P(None, "tp"),
        P("sp", None, "tp"),
        P(None, "tp", None),
        P(),
        P(),
        P("sp", None),
        P("sp", None),
        P("sp", None, "tp"),
        P("sp", None, "tp"),
        P("sp", "tp", None),
        P(),
        P(),
        P(),
        P(),
        P(),
    )
    out_specs = P(("sp", "tp"), None)
    return jax.shard_map(shards, mesh=mesh, in_specs=in_specs, out_specs=out_specs, check_vma=False)
```

profile of v0, /device:TPU:0, one launch (start us, length us, event | category | flops | bytes accessed | tf_op | source)
XLA Modules:
  0.0 279.8 jit_solution(14825979495545333488)
XLA Ops:
  7.6 4.9 %collective-permute-start = (bf16[3,2,256]{2,0,1:T(4,128)(2,1)S(1)}, bf16[3,2,256]{2,0,1:T(4,128)(2,1)S(1)}, u32[]{:S(2)}, u32[]{:S(2)}) collective-permute-start(bf16[3,2,256]{2,0,1:T(4,128)(2,1)S(1)} %slice.292), channel_id=1, source_target_pairs={{0,4},{4,8},{8,12},{12,16},{16,20},{20,24},{24,28},{1,5},{5,9},{9,... | collective-permute-start | bytes 9224 | tf_op jit(solution)/shard_map/ppermute | solution.py:26
  22.3 26.5 %all-gather.1 = f32[8,2,256]{2,1,0:T(2,128)S(1)} all-gather(f32[1,2,256]{2,1,0:T(2,128)S(1)} %bitcast.154), channel_id=2, replica_groups=mesh['sp'=8,'tp'=4] {'sp'}, dimensions={0}, use_global_device_ids=true | all-gather | bytes 18432 | tf_op jit(solution)/shard_map/all_gather | solution.py:12
  48.8 26.2 %all_gather.13 = f32[8,2,256]{2,1,0:T(2,128)S(1)} all-gather(f32[1,2,256]{2,1,0:T(2,128)} %get-tuple-element.64), channel_id=1, replica_groups=mesh['sp'=8,'tp'=4] {'sp'}, dimensions={0}, use_global_device_ids=true | all-gather | bytes 18432 | tf_op jit(solution)/shard_map/all_gather | solution.py:12
  78.0 1.3 fusion.5
  80.2 2.4 scatter_custom_fusion
  82.8 15.6 %reduce-scatter.3.cloned.1.call-done = bf16[32,2048]{1,0:T(8,128)(2,1)} async-done(((bf16[128,2048]{1,0:T(8,128)(2,1)}), bf16[32,2048]{1,0:T(8,128)(2,1)}) %reduce-scatter.3.cloned.1.call-update) | async-done | bytes 131088 | tf_op jit(solution)/shard_map/reduce_scatter | solution.py:116
  102.3 6.6 %all_gather.16 = bf16[128,2048]{1,0:T(8,128)(2,1)S(1)} all-gather(bf16[32,2048]{1,0:T(8,128)(2,1)S(1)} %add_convert_fusion.1), channel_id=1, replica_groups=mesh['sp'=8,'tp'=4] {'tp'}, dimensions={0}, use_global_device_ids=true | all-gather | bytes 655360 | tf_op jit(solution)/shard_map/all_gather | solution.py:144
  109.0 4.1 %gather_fusion = bf16[640,2048]{1,0:T(8,128)(2,1)} fusion(bf16[129,2048]{1,0:T(8,128)(2,1)S(1)} %concatenate.35, s32[1024]{0:T(1024)S(1)} %pad_clamp_fusion.1), kind=kCustom, calls=%fused_computation | custom fusion | bytes 5245440 | tf_op jit(solution)/shard_map/jit(_take)/gather | solution.py:154
  113.1 5.1 %gather.10 = bf16[8,4,20,2048]{3,2,1,0:T(8,128)(2,1)} reshape(bf16[640,2048]{1,0:T(8,128)(2,1)} %gather_fusion) | data formatting | bytes 5242880 | tf_op jit(solution)/shard_map/jit(_take)/gather | solution.py:154
  118.2 2.2 broadcast_select_fusion
  120.5 2.1 copy.103
  122.6 65.4 %all_to_all.10 = bf16[8,4,20,2048]{3,1,2,0:T(4,128)(2,1)S(1)} all-to-all(bf16[8,4,20,2048]{3,1,2,0:T(4,128)(2,1)S(1)} %copy.103), channel_id=1, replica_groups=mesh['sp'=8,'tp'=4] {'sp'}, dimensions={0} | all-to-all | bytes 5242880 | tf_op jit(solution)/shard_map/all_to_all | solution.py:155
  188.0 1.5 copy-done.1
  189.5 1.9 fusion.7
  191.4 6.8 %fusion.4 = bf16[8,1,4,20,2048]{4,3,2,0,1:T(8,128)(2,1)} fusion(bf16[8,4,20,2048]{3,1,2,0:T(4,128)(2,1)} %copy-done.1, bf16[1,128,2048]{2,1,0:T(8,128)(2,1)S(1)} %copy-done.7, bf16[1,2048,128]{2,1,0:T(8,128)(2,1)S(1)} %copy-done.8, f32[8,1,4,20,128]{4,3,2,0,1:T(8,128)S(1)} %fusion.7), kind=kOutput, calls=%fused_computation.11 | convolution fusion | flops 672890880 | bytes 6619136 | tf_op jit(solution)/shard_map/slxcf,lfd->slxcd/dot_general | solution.py:59
  198.3 4.9 %copy.106 = bf16[8,1,4,20,2048]{4,0,3,1,2:T(8,128)(2,1)} copy(bf16[8,1,4,20,2048]{4,3,2,0,1:T(8,128)(2,1)} %fusion.4) | data formatting | bytes 5242880 | tf_op jit(solution)/shard_map/convert_element_type | solution.py:162
  203.2 33.3 %reduce-scatter.5.cloned.1.call-done = bf16[8,1,1,20,2048]{4,0,3,1,2:T(8,128)(2,1)} async-done(((bf16[8,1,4,20,2048]{4,0,3,1,2:T(8,128)(2,1)}), bf16[8,1,1,20,2048]{4,0,3,1,2:T(8,128)(2,1)}) %reduce-scatter.5.cloned.1.call-update) | async-done | bytes 655376 | tf_op jit(solution)/shard_map/reduce_scatter | solution.py:161
  236.5 2.4 copy.107
  238.9 5.5 %all-to-all-start.1 = ((bf16[8,1,20,2048]{3,2,1,0:T(8,128)(2,1)}), bf16[8,1,20,2048]{3,2,1,0:T(8,128)(2,1)S(1)}, u32[]{:S(2)}, u32[]{:S(2)}) async-start(bf16[8,1,20,2048]{3,2,1,0:T(8,128)(2,1)} %copy.107), calls=%async_computation.3 | async-start | bytes 1572864 | tf_op jit(solution)/shard_map/all_to_all | solution.py:165
  245.8 2.7 fusion.114
  248.5 16.0 %all-to-all-done.1 = bf16[8,1,20,2048]{3,2,1,0:T(8,128)(2,1)S(1)} async-done(((bf16[8,1,20,2048]{3,2,1,0:T(8,128)(2,1)}), bf16[8,1,20,2048]{3,2,1,0:T(8,128)(2,1)S(1)}, u32[]{:S(2)}, u32[]{:S(2)}) %all-to-all-start.1) | async-done | bytes 655392 | tf_op jit(solution)/shard_map/all_to_all | solution.py:165
  264.6 1.8 gather_fusion.1
  266.5 1.4 reshape.189
  268.6 3.3 %fusion.113 = (f32[32]{0:T(128)S(1)}, f32[32,2048]{1,0:T(8,128)S(1)}) fusion(f32[32,2048]{1,0:T(8,128)S(1)} %multiply_reduce_fusion, bf16[512,2048]{1,0:T(8,128)(2,1)} %param.41, bf16[32,2048]{1,0:T(8,128)(2,1)S(1)} %copy-done.4, bf16[2048,512]{1,0:T(8,128)(2,1)} %param.40, f32[32,512]{1,0:T(8,128)} %fusion.114), kind=kOutput, calls=%fused_computation.182 | convolution fusion | flops 134643680 | bytes 4915328 | tf_op jit(solution)/shard_map/dot_general | solution.py:177
  (189 shorter events, 21.5 us)
Async XLA Ops:
  6.5 71.4 %copy-start = (bf16[2,256,2048]{2,1,0:T(8,128)(2,1)S(1)}, bf16[2,256,2048]{2,1,0:T(8,128)(2,1)}, u32[]{:S(2)}) copy-start(bf16[2,256,2048]{2,1,0:T(8,128)(2,1)} %param.31) | copy-start | bytes 6291460
  6.5 9.5 %copy-start.24 = (bf16[2,2,128,128]{3,2,1,0:T(8,128)(2,1)S(1)}, bf16[2,2,128,128]{3,2,1,0:T(8,128)(2,1)}, u32[]{:S(2)}) copy-start(bf16[2,2,128,128]{3,2,1,0:T(8,128)(2,1)} %param.28) | copy-start | bytes 393220
  6.5 10.1 %copy-start.25 = (bf16[2,4,64,64]{3,2,1,0:T(8,128)(2,1)S(1)}, bf16[2,4,64,64]{3,2,1,0:T(8,128)(2,1)}, u32[]{:S(2)}) copy-start(bf16[2,4,64,64]{3,2,1,0:T(8,128)(2,1)} %param.27) | copy-start | bytes 196612
  6.5 91.9 %reduce-scatter.3.cloned.1.call-start = ((), (), s32[]{:S(2)}) async-start(), calls=%async_computation.4 | async-start | bytes 655360 | tf_op jit(solution)/shard_map/reduce_scatter | solution.py:116
  7.6 8.1 %collective-permute-start = (bf16[3,2,256]{2,0,1:T(4,128)(2,1)S(1)}, bf16[3,2,256]{2,0,1:T(4,128)(2,1)S(1)}, u32[]{:S(2)}, u32[]{:S(2)}) collective-permute-start(bf16[3,2,256]{2,0,1:T(4,128)(2,1)S(1)} %slice.292), channel_id=1, source_target_pairs={{0,4},{4,8},{8,12},{12,16},{16,20},{20,24},{24,28},{1,5},{5,9},{9,... | collective-permute-start | bytes 9224 | tf_op jit(solution)/shard_map/ppermute | solution.py:26
  13.2 2.8 %copy-start.12 = (f32[2,256]{1,0:T(2,128)}, f32[2,256]{1,0:T(2,128)S(1)}, u32[]{:S(2)}) copy-start(f32[2,256]{1,0:T(2,128)S(1)} %get-tuple-element.84) | copy-start | bytes 6148
  13.2 2.8 %copy-start.13 = (f32[2,256]{1,0:T(2,128)}, f32[2,256]{1,0:T(2,128)S(1)}, u32[]{:S(2)}) copy-start(f32[2,256]{1,0:T(2,128)S(1)} %get-tuple-element.85) | copy-start | bytes 6148
  13.2 2.8 %copy-start.14 = (f32[2,256]{1,0:T(2,128)}, f32[2,256]{1,0:T(2,128)S(1)}, u32[]{:S(2)}) copy-start(f32[2,256]{1,0:T(2,128)S(1)} %get-tuple-element.86) | copy-start | bytes 6148
  13.2 2.8 %copy-start.15 = (f32[2,256]{1,0:T(2,128)}, f32[2,256]{1,0:T(2,128)S(1)}, u32[]{:S(2)}) copy-start(f32[2,256]{1,0:T(2,128)S(1)} %get-tuple-element.87) | copy-start | bytes 6148
  77.9 2.1 copy-start.11
  77.9 20.6 %copy-start.5 = (bf16[32,2048]{1,0:T(8,128)(2,1)S(1)}, bf16[32,2048]{1,0:T(8,128)(2,1)}, u32[]{:S(2)}) copy-start(bf16[32,2048]{1,0:T(8,128)(2,1)} %param.23) | copy-start | bytes 393220
  78.0 22.6 %copy-start.17 = (f32[2048]{0:T(1024)S(1)}, f32[2048]{0:T(1024)}, u32[]{:S(2)}) copy-start(f32[2048]{0:T(1024)} %param.33) | copy-start | bytes 24580
  78.0 22.6 %copy-start.18 = (f32[2048]{0:T(1024)S(1)}, f32[2048]{0:T(1024)}, u32[]{:S(2)}) copy-start(f32[2048]{0:T(1024)} %param.32) | copy-start | bytes 24580
  79.4 157.1 %reduce-scatter.5.cloned.1.call-start = ((), (), s32[]{:S(2)}) async-start(), calls=%async_computation.5 | async-start | bytes 3276800 | tf_op jit(solution)/shard_map/reduce_scatter | solution.py:161
  80.2 21.5 %copy-start.16 = (s32[4,128]{1,0:T(4,128)}, s32[4,128]{1,0:T(4,128)S(1)}, u32[]{:S(2)}) copy-start(s32[4,128]{1,0:T(4,128)S(1)} %select_reduce_fusion) | copy-start | bytes 6148
  122.5 66.9 %copy-start.23 = (bf16[1,2048,128]{2,1,0:T(8,128)(2,1)S(1)}, bf16[1,2048,128]{2,1,0:T(8,128)(2,1)}, u32[]{:S(2)}) copy-start(bf16[1,2048,128]{2,1,0:T(8,128)(2,1)} %param.36) | copy-start | bytes 1572868
  189.5 1.9 copy-start.7
  189.5 1.9 copy-start.8
  203.2 41.2 %copy-start.22 = (f32[128,4]{0,1:T(4,128)S(1)}, f32[128,4]{0,1:T(4,128)}, u32[]{:S(2)}) copy-start(f32[128,4]{0,1:T(4,128)} %param.35) | copy-start | bytes 6148
  203.2 42.7 %copy-start.3 = (bf16[32,2048]{1,0:T(8,128)(2,1)S(1)}, bf16[32,2048]{1,0:T(8,128)(2,1)}, u32[]{:S(2)}) copy-start(bf16[32,2048]{1,0:T(8,128)(2,1)} %copy-done.2) | copy-start | bytes 393220
  238.9 25.6 %all-to-all-start.1 = ((bf16[8,1,20,2048]{3,2,1,0:T(8,128)(2,1)}), bf16[8,1,20,2048]{3,2,1,0:T(8,128)(2,1)S(1)}, u32[]{:S(2)}, u32[]{:S(2)}) async-start(bf16[8,1,20,2048]{3,2,1,0:T(8,128)(2,1)} %copy.107), calls=%async_computation.3 | async-start | bytes 1572864 | tf_op jit(solution)/shard_map/all_to_all | solution.py:165
  266.5 2.1 copy-start.4
  268.6 3.5 %copy-start.19 = (f32[2048]{0:T(1024)S(1)}, f32[2048]{0:T(1024)}, u32[]{:S(2)}) copy-start(f32[2048]{0:T(1024)} %param.43) | copy-start | bytes 24580
  268.6 3.5 %copy-start.20 = (f32[2048]{0:T(1024)S(1)}, f32[2048]{0:T(1024)}, u32[]{:S(2)}) copy-start(f32[2048]{0:T(1024)} %param.42) | copy-start | bytes 24580
  (6 other events, 8.3 us)
Sparse Core Ops, SparseCore 0:
  79.5 18.9 reduce-scatter.2
  203.3 33.1 reduce-scatter.4
where the time goes:
time: 281 us; the launch traced here: 280 us
  blocking collectives  125 us (44%)
  waiting for transfers between devices  64.9 us (23%)
  local copies, waits for them, and re-layouts  33.7 us (12%)
  matrix products  16.6 us (6%)
  other arithmetic  15.2 us (5%)
  between operations  14.3 us (5%)
  starting transfers between devices  10.4 us (4%)
    all_to_all x1, blocking collectives, shards(): lax.all_to_all(outgoing, 'sp', split_axis=0, concat_axis=0, tiled=True)  65.4 us
    all_gather x2, blocking collectives, entering(): gathered = jax.tree.map(lambda a: lax.all_gather(a, axis), part)  52.7 us
    reduce_scatter x1, waiting for transfers between devices, shards(): lax.psum_scatter(partial_value.astype(jnp.bfloat16), 'tp', scatter_dimens...  33.3 us
    all_to_all x1, waiting for transfers between devices, shards(): lax.all_to_all(leaving, 'sp', split_axis=0, concat_axis=0, tiled=True)  16 us
    reduce_scatter x1, waiting for transfers between devices, shards(): lax.psum_scatter(jnp.einsum('tgc,gcd->td', branch_output, recurrence_outp...  15.6 us
    gather x2, local copies, waits for them, and re-layouts, shards(): jnp.take(padded_rows, table, axis=0)  9.28 us
    dot_general x1, matrix products, expert_terms(): jnp.einsum(down_form, hidden, down_w, preferred_element_type=jnp.float32)  6.84 us
    all_gather x1, blocking collectives, shards(): gathered = lax.all_gather(normed, 'tp', axis=0, tiled=True)  6.58 us
  transfers between devices with their start and end apart: 4, of which 3 were waited for; matrix products, arithmetic and copies ran while one was open for 4% of the time, Pallas kernels for 0%

commit v1 on v0

v1 whole, which is shorter than its diff:
```python
import functools

import jax
import jax.numpy as jnp
from jax import lax
from jax.experimental import pallas as pl
from jax.experimental.pallas import tpu as pltpu
from jax.sharding import PartitionSpec as P

RESIDUAL_SCALE = 8.0**0.25
NORM_EPSILON = 1e-05
LANES = 128
MESH = pl.DeviceIdType.MESH
F32 = jnp.float32
BF16 = jnp.bfloat16


def layer_norm(values, gain, bias):
    row_mean = jnp.mean(values, axis=-1, keepdims=True)
    spread = jnp.mean(jnp.square(values - row_mean), axis=-1, keepdims=True)
    return (values - row_mean) * lax.rsqrt(spread + NORM_EPSILON) * gain + bias


def expm1_negative(z):
    small = jnp.full_like(z, 1.0 / 40320.0)
    for n in (5040.0, 720.0, 120.0, 24.0, 6.0, 2.0, 1.0):
        small = small * z + 1.0 / n
    return jnp.where(z > -0.5, small * z, jnp.exp(z) - 1.0)


def silu(v):
    return v * jax.nn.sigmoid(v)


def dot(a, b):
    return jnp.dot(a, b, preferred_element_type=F32)


def kernel(
    dims,
    stream, rec_in, gate_in, taps, gates, rate, extra, n1g, n1b, n2g, n2b, wdense,
    out_w_hbm, rg_hbm, ru_hbm, rd_hbm, sg_hbm, su_hbm, sd_hbm,
    result,
    padded, halo, carry_own, carry_in, w_own, w_in, out_w, w_gu, w_d, s_gu, s_d,
    part, part_in, rows, hid, y_part, x_in, z_out, z_in, moe,
    local_sem, halo_sem, carry_send, carry_recv, w_send, w_recv,
    wt_send, wt_recv, tp_send, tp_recv, ag_send, ag_recv, fw_send, fw_recv,
    xs_send, xs_recv, zs_send, zs_recv,
):
    sp_n, tp_n, inner = dims
    outer = sp_n // inner
    pairs = tp_n // 2
    sp, tp = lax.axis_index("sp"), lax.axis_index("tp")
    zi, xi = sp // inner, lax.rem(sp, inner)
    other_x = lax.rem(xi + 1, inner)
    x_peer = zi * inner + other_x
    half_c = lax.rem(tp, 2)
    yi = tp // 2
    mate = yi * 2 + (1 - half_c)
    length, chans = rec_in.shape
    quarter = stream.shape[0]
    fe = rg_hbm.shape[1]
    fs = sg_hbm.shape[1]

    def remote(src, dst, send, recv, where):
        return pltpu.make_async_remote_copy(
            src_ref=src, dst_ref=dst, send_sem=send, recv_sem=recv,
            device_id=where, device_id_type=MESH,
        )

    locals_ = [
        pltpu.make_async_copy(rg_hbm, w_gu.at[tp, :, pl.ds(0, fe)], local_sem.at[0]),
        pltpu.make_async_copy(ru_hbm, w_gu.at[tp, :, pl.ds(fe, fe)], local_sem.at[1]),
        pltpu.make_async_copy(rd_hbm, w_d.at[tp], local_sem.at[2]),
        pltpu.make_async_copy(out_w_hbm, out_w, local_sem.at[3]),
        pltpu.make_async_copy(sg_hbm, s_gu.at[:, pl.ds(0, fs)], local_sem.at[4]),
        pltpu.make_async_copy(su_hbm, s_gu.at[:, pl.ds(fs, fs)], local_sem.at[5]),
        pltpu.make_async_copy(sd_hbm, s_d, local_sem.at[6]),
    ]

    halo_copy = remote(
        rec_in.at[pl.ds(length - 16, 16)], halo, halo_sem.at[0], halo_sem.at[1],
        (lax.rem(sp + 1, sp_n), tp),
    )
    halo_copy.start()

    def weight_dst(slot, kind):
        if kind == 0:
            return w_gu.at[slot, :, pl.ds(0, fe)]
        if kind == 1:
            return w_gu.at[slot, :, pl.ds(fe, fe)]
        return w_d.at[slot]

    sources = (rg_hbm, ru_hbm, rd_hbm)

    def weight_out(kind, step):
        return remote(
            sources[kind], weight_dst(tp, kind),
            wt_send.at[kind, step], wt_recv.at[kind, tp],
            (sp, lax.rem(yi + step, pairs) * 2 + half_c),
        )

    def weight_mate(kind, slot, step):
        src = sources[kind] if step == 0 else weight_dst(slot, kind)
        return remote(
            src, weight_dst(slot, kind),
            wt_send.at[kind, pairs + step], wt_recv.at[kind, slot], (sp, mate),
        )

    def pair_slot(step):
        return lax.rem(yi + step, pairs) * 2 + half_c

    for kind in range(3):
        for step in range(1, pairs):
            weight_out(kind, step).start()
    locals_[3].start()
    for kind in range(3):
        weight_mate(kind, tp, 0).start()
        locals_[kind].start()
    for i in (4, 5, 6):
        locals_[i].start()

    w_own_copy = pltpu.make_async_copy(wdense, w_in.at[sp], local_sem.at[7])
    w_own_copy.start()

    def w_out(step):
        return remote(
            wdense, w_in.at[sp], w_send.at[step], w_recv.at[sp], (lax.rem(sp + step, sp_n), tp)
        )

    @pl.loop(1, sp_n)
    def _(step):
        w_out(step).start()

    padded[pl.ds(8, length)] = rec_in[...].astype(F32)
    halo_copy.wait()
    border = halo[...].astype(F32)[8:16]
    padded[pl.ds(0, 8)] = jnp.where(sp > 0, border, jnp.zeros_like(border))
    tap_n = taps.shape[0]
    summed = taps[0:1] * padded[pl.ds(8 - tap_n + 1, length)]
    for k in range(1, tap_n):
        summed = summed + taps[k : k + 1] * padded[pl.ds(8 - tap_n + 1 + k, length)]
    conv = summed.astype(BF16)
    half = chans // 2
    first = dot(conv[:, :half], gates[0])
    second = dot(conv[:, half:], gates[1])
    recur = jax.nn.sigmoid(jnp.concatenate([first[:, :half], second[:, :half]], axis=1))
    inp = jax.nn.sigmoid(jnp.concatenate([first[:, half:], second[:, half:]], axis=1))
    log_decay = recur * rate[...] + extra[...]
    decay = jnp.exp(log_decay)
    state = jnp.sqrt(-expm1_negative(2.0 * log_decay)) * inp * conv.astype(F32)
    row_id = lax.broadcasted_iota(jnp.int32, (length, chans), 0)
    shift = 1
    while shift < length:
        live = row_id >= shift
        before_a = jnp.where(live, pltpu.roll(decay, shift, 0), 1.0)
        before_b = jnp.where(live, pltpu.roll(state, shift, 0), 0.0)
        state = decay * before_b + state
        decay = decay * before_a
        shift *= 2
    carry_own[...] = jnp.concatenate(
        [decay[length - 1 :], state[length - 1 :], jnp.zeros((6, chans), F32)], axis=0
    )

    def carry_out(step):
        return remote(
            carry_own, carry_in.at[sp], carry_send.at[step], carry_recv.at[sp],
            (lax.rem(sp + step, sp_n), tp),
        )

    def carry_arrival(who):
        return remote(
            carry_own, carry_in.at[who], carry_send.at[0], carry_recv.at[who], (sp, tp)
        )

    @pl.loop(1, sp_n)
    def _(step):
        carry_out(step).start()

    gi = gate_in[...].astype(F32)
    gelu = 0.5 * gi * (1.0 + jnp.tanh(0.7978845608028654 * (gi + 0.044715 * gi * gi * gi)))

    @pl.loop(1, sp_n)
    def _(step):
        carry_arrival(lax.rem(sp + step, sp_n)).wait_recv()

    carry_in[sp] = carry_own[...]

    def fold(who, incoming):
        link = carry_in[who]
        return jnp.where(who < sp, link[0:1] * incoming + link[1:2], incoming)

    incoming = lax.fori_loop(0, sp_n, fold, jnp.zeros((1, chans), F32))
    branch = (gelu * (state + decay * incoming)).astype(BF16)
    locals_[3].wait()
    part[...] = dot(branch, out_w[...]).astype(BF16).reshape(part.shape)

    def part_out(step):
        to = lax.rem(tp + step, tp_n)
        return remote(
            part.at[to], part_in.at[tp], tp_send.at[step], tp_recv.at[tp], (sp, to)
        )

    def part_arrival(who):
        return remote(part.at[who], part_in.at[who], tp_send.at[0], tp_recv.at[who], (sp, tp))

    for step in range(1, tp_n):
        part_out(step).start()
    mixed = part[tp].astype(F32)
    for step in range(1, tp_n):
        who = lax.rem(tp + step, tp_n)
        part_arrival(who).wait_recv()
        mixed = mixed + part_in[who].astype(F32)
    normed = layer_norm(
        RESIDUAL_SCALE * stream[...].astype(F32) + mixed, n1g[...], n1b[...]
    ).astype(BF16)
    rows[sp] = normed

    def ag_out(step):
        return remote(
            rows.at[sp], rows.at[sp], ag_send.at[step], ag_recv.at[sp],
            (lax.rem(zi + step, outer) * inner + xi, tp),
        )

    def ag_arrival(who):
        return remote(rows.at[who], rows.at[who], ag_send.at[0], ag_recv.at[who], (sp, tp))

    def forward(who):
        return remote(
            rows.at[who], rows.at[who], fw_send.at[who], ag_recv.at[who], (x_peer, tp)
        )

    @pl.loop(1, outer)
    def _(step):
        ag_out(step).start()

    forward(sp).start()

    def weight_arrival(kind, slot):
        return remote(
            weight_dst(slot, kind), weight_dst(slot, kind),
            wt_send.at[kind, 0], wt_recv.at[kind, slot], (sp, mate),
        )

    locals_[4].wait()
    locals_[5].wait()
    locals_[6].wait()
    up = dot(normed, s_gu[...])
    s_hid = (silu(up[:, :fs]) * up[:, fs:]).astype(BF16)
    moe[...] = dot(s_hid, s_d[...]) + RESIDUAL_SCALE * normed.astype(F32)

    @pl.loop(1, sp_n)
    def _(step):
        who = lax.rem(sp + step, sp_n)
        remote(wdense, w_in.at[who], w_send.at[0], w_recv.at[who], (sp, tp)).wait_recv()

    w_own_copy.wait()
    for kind in range(3):
        for step in range(1, pairs):
            weight_arrival(kind, pair_slot(step)).wait_recv()
            weight_mate(kind, pair_slot(step), step).start()
    for kind in range(3):
        locals_[kind].wait()
        for step in range(pairs):
            weight_arrival(kind, lax.rem(yi + step, pairs) * 2 + 1 - half_c).wait_recv()

    width = stream.shape[1]
    grp = inner * quarter

    def x_out(zj):
        return remote(
            y_part.at[zj * inner + other_x], x_in.at[zj], xs_send.at[zj], xs_recv.at[zj],
            (x_peer, tp),
        )

    @pl.loop(0, outer)
    def _(step):
        zj = lax.rem(zi + step, outer)
        mine, theirs = zj * inner + xi, zj * inner + other_x

        @pl.when(step > 0)
        def _():
            ag_arrival(mine).wait_recv()
            forward(mine).start()

        ag_arrival(theirs).wait_recv()
        block = rows[pl.ds(zj * inner, inner)].reshape(grp, width)
        for t in range(tp_n):
            gu = dot(block, w_gu[t])
            hid[:, t * fe : (t + 1) * fe] = (silu(gu[:, :fe]) * gu[:, fe:]).astype(BF16)
        wv = w_in[pl.ds(zj * inner, inner)].reshape(grp, w_in.shape[2])
        lane = lax.broadcasted_iota(jnp.int32, wv.shape, 1)
        weight = jnp.sum(jnp.where(lane == sp, wv, 0.0), axis=1, keepdims=True)
        value = weight * dot(hid[...], w_d[...].reshape(tp_n * fe, width))
        y_part[pl.ds(zj * inner, inner)] = value.astype(BF16).reshape(inner, quarter, width)
        x_out(zj).start()

    def z_send(step):
        zj = lax.rem(zi + step, outer)
        return remote(
            z_out.at[zj], z_in.at[zi], zs_send.at[step], zs_recv.at[zi], (zj * inner + xi, tp)
        )

    @pl.loop(1, outer)
    def _(step):
        zj = lax.rem(zi + step, outer)
        x_out(zj).wait_recv()
        both = y_part[zj * inner + xi].astype(F32) + x_in[zj].astype(F32)
        z_out[zj] = both.astype(BF16)
        z_send(step).start()

    x_out(zi).wait_recv()
    moe[...] += y_part[sp].astype(F32) + x_in[zi].astype(F32)

    @pl.loop(1, outer)
    def _(step):
        zj = lax.rem(zi + step, outer)
        remote(z_out.at[zj], z_in.at[zj], zs_send.at[0], zs_recv.at[zj], (sp, tp)).wait_recv()
        moe[...] += z_in[zj].astype(F32)

    result[...] = layer_norm(moe[...], n2g[...], n2b[...]).astype(BF16)

    for kind in range(3):
        for step in range(1, pairs):
            weight_out(kind, step).wait_send()
            weight_mate(kind, pair_slot(step), step).wait_send()
        weight_mate(kind, tp, 0).wait_send()
    for step in range(1, tp_n):
        part_out(step).wait_send()

    @pl.loop(1, sp_n)
    def _(step):
        w_out(step).wait_send()
        carry_out(step).wait_send()

    @pl.loop(1, outer)
    def _(step):
        ag_out(step).wait_send()
        z_send(step).wait_send()

    @pl.loop(0, outer)
    def _(step):
        forward(step * inner + xi).wait_send()
        x_out(step).wait_send()


def block_diagonal(maps):
    kinds, heads, size, _ = maps.shape
    eye = jnp.eye(heads, dtype=maps.dtype)
    spread = maps[:, :, :, None, :] * eye[None, :, None, :, None]
    spread = spread.reshape(kinds, heads * size, heads * size)
    return jnp.concatenate([spread[i] for i in range(kinds)], axis=1)


def shards(
    dims,
    stream,
    recurrence_input,
    output_gate_input,
    convolution_taps,
    first_group_gates,
    second_group_gates,
    channel_decay,
    position_log_extra,
    recurrence_output_weight,
    first_norm_gain,
    first_norm_bias,
    routed_expert_index,
    routed_expert_weight,
    routed_gate_weight,
    routed_up_weight,
    routed_down_weight,
    shared_gate_weight,
    shared_up_weight,
    shared_down_weight,
    second_norm_gain,
    second_norm_bias,
):
    sp_n, tp_n, inner = dims
    outer = sp_n // inner
    length = recurrence_input.shape[0]
    chans = 2 * recurrence_input.shape[2]
    quarter, width = stream.shape
    fe = routed_gate_weight.shape[2]
    fs = shared_gate_weight.shape[1]
    lanes = -(-sp_n // LANES) * LANES
    flat = lambda a: a.reshape(a.shape[0], chans)
    gates = jnp.stack([block_diagonal(first_group_gates), block_diagonal(second_group_gates)])
    rate = (-8.0 * jax.nn.softplus(-channel_decay)).reshape(1, chans)
    own = lax.axis_index("tp") * quarter
    ids = lax.dynamic_slice_in_dim(routed_expert_index, own, quarter, 0)
    wts = lax.dynamic_slice_in_dim(routed_expert_weight, own, quarter, 0)
    hits = ids[:, :, None] == jnp.arange(lanes, dtype=jnp.int32)[None, None, :]
    wdense = jnp.sum(jnp.where(hits, wts[:, :, None], 0.0), axis=1)
    vec = lambda a: a.reshape(1, width)
    vmem = pl.BlockSpec(memory_space=pltpu.VMEM)
    hbm = pl.BlockSpec(memory_space=pl.ANY)
    dma = pltpu.SemaphoreType.DMA
    block = (quarter, width)
    pairs = tp_n // 2
    return pl.pallas_call(
        functools.partial(kernel, dims),
        out_shape=jax.ShapeDtypeStruct(block, BF16),
        in_specs=[vmem] * 12 + [hbm] * 7,
        out_specs=vmem,
        scratch_shapes=[
            pltpu.VMEM((length + 8, chans), F32),
            pltpu.VMEM((16, chans), BF16),
            pltpu.VMEM((8, chans), F32),
            pltpu.VMEM((sp_n, 8, chans), F32),
            pltpu.VMEM((8, LANES), F32),
            pltpu.VMEM((sp_n, quarter, lanes), F32),
            pltpu.VMEM((chans, width), BF16),
            pltpu.VMEM((tp_n, width, 2 * fe), BF16),
            pltpu.VMEM((tp_n, fe, width), BF16),
            pltpu.VMEM((width, 2 * fs), BF16),
            pltpu.VMEM((fs, width), BF16),
            pltpu.VMEM((tp_n,) + block, BF16),
            pltpu.VMEM((tp_n,) + block, BF16),
            pltpu.VMEM((sp_n,) + block, BF16),
            pltpu.VMEM((inner * quarter, tp_n * fe), BF16),
            pltpu.VMEM((sp_n,) + block, BF16),
            pltpu.VMEM((outer,) + block, BF16),
            pltpu.VMEM((outer,) + block, BF16),
            pltpu.VMEM((outer,) + block, BF16),
            pltpu.VMEM(block, F32),
            dma((8,)),
            dma((2,)),
            dma((sp_n,)),
            dma((sp_n,)),
            dma((sp_n,)),
            dma((sp_n,)),
            dma((3, 2 * pairs)),
            dma((3, tp_n)),
            dma((tp_n,)),
            dma((tp_n,)),
            dma((outer,)),
            dma((sp_n,)),
            dma((sp_n,)),
            dma((1,)),
            dma((outer,)),
            dma((outer,)),
            dma((outer,)),
            dma((outer,)),
        ],
        compiler_params=pltpu.CompilerParams(
            has_side_effects=True, vmem_limit_bytes=60 * 2**20
        ),
    )(
        stream,
        flat(recurrence_input),
        flat(output_gate_input),
        flat(convolution_taps).astype(F32),
        gates,
        rate,
        flat(position_log_extra),
        vec(first_norm_gain),
        vec(first_norm_bias),
        vec(second_norm_gain),
        vec(second_norm_bias),
        wdense,
        recurrence_output_weight.reshape(chans, width),
        routed_gate_weight.reshape(width, fe),
        routed_up_weight.reshape(width, fe),
        routed_down_weight.reshape(fe, width),
        shared_gate_weight,
        shared_up_weight,
        shared_down_weight,
    )


def solution(mesh):
    in_specs = (
        P(("sp", "tp"), None),
        P("sp", None, "tp"),
        P("sp", None, "tp"),
        P(None, None, "tp"),
        P(None, "tp", None, None),
        P(None, "tp", None, None),
        P(None, "tp"),
        P("sp", None, "tp"),
        P(None, "tp", None),
        P(),
        P(),
        P("sp", None),
        P("sp", None),
        P("sp", None, "tp"),
        P("sp", None, "tp"),
        P("sp", "tp", None),
        P(),
        P(),
        P(),
        P(),
        P(),
    )
    dims = (mesh.shape["sp"], mesh.shape["tp"], 2)
    return jax.shard_map(
        functools.partial(shards, dims),
        mesh=mesh,
        in_specs=in_specs,
        out_specs=P(("sp", "tp"), None),
        check_vma=False,
    )
```

time: 281 us -> 108 us (0.38)
  blocking collectives: 125 us -> 0 us
  Pallas kernels: 0 us -> 97.6 us
  waiting for transfers between devices: 64.9 us -> 0 us
  local copies, waits for them, and re-layouts: 33.7 us -> 7.17 us
  matrix products: 16.6 us -> 0 us
  between operations: 14.3 us -> 0.13 us
  other arithmetic: 15.2 us -> 3.13 us
  starting transfers between devices: 10.4 us -> 0 us
    pallas_call x0 -> x1, Pallas kernels: none -> 97.6 us  [shards(): pl.pallas_call(functools.partial(kernel, dims), out_shape=jax.ShapeDtypeS...]
    all_to_all x1 -> x0, blocking collectives: 65.4 us -> none  [shards(): lax.all_to_all(outgoing, 'sp', split_axis=0, concat_axis=0, tiled=True)]
    all_gather x3 -> x0, blocking collectives: 59.3 us -> none  [the longest x2 52.7 us: entering(): gathered = jax.tree.map(lambda a: lax.all_gather(a, axis), part)]
    reduce_scatter x2 -> x0, waiting for transfers between devices: 48.9 us -> none  [the longest x1 33.3 us: shards(): lax.psum_scatter(partial_value.astype(jnp.bfloat16), 'tp', scatter_dimens...]
    dot_general x7 -> x0, matrix products: 16.6 us -> none  [the longest x1 6.84 us: expert_terms(): jnp.einsum(down_form, hidden, down_w, preferred_element_type=jnp.float32)]
    all_to_all x1 -> x0, waiting for transfers between devices: 16 us -> none  [shards(): lax.all_to_all(leaving, 'sp', split_axis=0, concat_axis=0, tiled=True)]
    gather x3 -> x0, local copies, waits for them, and re-layouts: 11.1 us -> none  [the longest x2 9.28 us: shards(): jnp.take(padded_rows, table, axis=0)]
    convert_element_type x2 -> x0, local copies, waits for them, and re-layouts: 6.3 us -> none  [the longest x1 4.9 us: shards(): partial_value.astype(jnp.bfloat16)]
  transfers between devices with their start and end apart: 4 -> 0, of which waited for: 3 -> 0; matrix products, arithmetic and copies ran while one was open for 4% -> 0% of each run, Pallas kernels for 0% -> 0%
where the time goes in v1:
time: 108 us
  Pallas kernels  97.6 us (90%)
  local copies, waits for them, and re-layouts  7.17 us (7%)
  other arithmetic  3.13 us (3%)
    pallas_call x1, Pallas kernels, shards(): pl.pallas_call(functools.partial(kernel, dims), out_shape=jax.ShapeDtypeS...  97.6 us
    unnamed x20, local copies, waits for them, and re-layouts  5.52 us

profile of v1, /device:TPU:0, one launch (start us, length us, event | category | flops | bytes accessed | tf_op | source)
XLA Modules:
  0.0 108.0 jit_solution(890034640013113857)
XLA Ops:
  0.0 0.0 copy-start
  0.0 0.7 copy-done
  0.7 0.1 constant_dynamic-slice_fusion
  0.8 0.8 constant_dynamic-slice_fusion.1
  1.5 0.7 select_reduce_fusion.wdense
  2.2 1.2 %broadcast_multiply_fusion.1 = bf16[2,2,128,2,128]{4,3,2,1,0:T(2,128)(2,1)S(1)} fusion(bf16[2,2]{1,0:T(2,128)(2,1)S(1)} %compare_convert_fusion, bf16[2,2,128,128]{3,2,1,0:T(8,128)(2,1)} %param.26), kind=kLoop, calls=%fused_computation.6 | loop fusion | flops 131072 | bytes 393224 | tf_op jit(solution)/shard_map/mul | solution.py:350
  3.4 0.2 fusion.4
  3.7 0.0 copy-start.1
  3.7 0.3 broadcast_multiply_fusion
  4.0 0.0 copy-start.3
  4.0 0.0 copy-start.4
  4.1 0.0 copy-start.5
  4.1 0.0 copy-start.6
  4.1 0.2 fusion.3
  4.3 0.2 squeeze.12
  4.5 0.2 squeeze.13
  4.7 0.8 pad_maximum_fusion.gates
  5.6 0.7 copy.30
  6.3 0.7 copy.24
  7.0 0.7 copy.25
  7.7 0.6 copy.26
  8.3 0.6 copy.29
  8.8 97.6 %shard_map.199 = bf16[32,2048]{1,0:T(8,128)(2,1)} custom-call(bf16[32,2048]{1,0:T(8,128)(2,1)} %stream.1, bf16[128,512]{1,0:T(8,128)(2,1)} %bitcast.35, bf16[128,512]{1,0:T(8,128)(2,1)} %bitcast.36, f32[4,512]{1,0:T(4,128)} %bitcast.45, bf16[2,256,512]{2,1,0:T(8,128)(2,1)} %pad_maximum_fusion.gates, f32[1,512]{1,0:T(1,128)} %bitcast.50, ...), custom_call_target="tpu_custom_call" | custom-call | tf_op jit(solution)/shard_map/pallas_call | solution.py:401
  106.4 1.6 %copy.34 = bf16[32,2048]{1,0:T(8,128)(2,1)} copy(bf16[32,2048]{1,0:T(8,128)(2,1)} %shard_map.199) | data formatting | bytes 262144
  (14 shorter events, 0.1 us)
Async XLA Ops:
  0.0 0.7 copy-start
  0.0 3.7 %copy-start.2 = (bf16[2,4,64,64]{3,2,1,0:T(8,128)(2,1)S(1)}, bf16[2,4,64,64]{3,2,1,0:T(8,128)(2,1)}, u32[]{:S(2)}) copy-start(bf16[2,4,64,64]{3,2,1,0:T(8,128)(2,1)} %param.25) | copy-start | bytes 196612
  3.7 1.9 %copy-start.1 = (f32[128,2,256]{2,1,0:T(2,128)S(1)}, f32[128,2,256]{2,1,0:T(2,128)}, u32[]{:S(2)}) copy-start(f32[128,2,256]{2,1,0:T(2,128)} %param.28) | copy-start | bytes 786436
  4.0 2.3 %copy-start.3 = (bf16[128,2,256]{2,1,0:T(2,128)(2,1)S(1)}, bf16[128,2,256]{2,1,0:T(2,128)(2,1)}, u32[]{:S(2)}) copy-start(bf16[128,2,256]{2,1,0:T(2,128)(2,1)} %param.22) | copy-start | bytes 393220
  4.0 2.9 %copy-start.4 = (bf16[128,2,256]{2,1,0:T(2,128)(2,1)S(1)}, bf16[128,2,256]{2,1,0:T(2,128)(2,1)}, u32[]{:S(2)}) copy-start(bf16[128,2,256]{2,1,0:T(2,128)(2,1)} %param.23) | copy-start | bytes 393220
  4.1 3.6 %copy-start.5 = (bf16[4,2,256]{2,1,0:T(2,128)(2,1)S(1)}, bf16[4,2,256]{2,1,0:T(2,128)(2,1)}, u32[]{:S(2)}) copy-start(bf16[4,2,256]{2,1,0:T(2,128)(2,1)} %param.24) | copy-start | bytes 12292
  4.1 4.2 %copy-start.6 = (f32[2,256]{1,0:T(2,128)S(1)}, f32[2,256]{1,0:T(2,128)}, u32[]{:S(2)}) copy-start(f32[2,256]{1,0:T(2,128)} %param.27) | copy-start | bytes 6148

commit v2 on v1

--- a/solution.py
+++ b/solution.py
@@ -10,6 +10,8 @@
 RESIDUAL_SCALE = 8.0**0.25
 NORM_EPSILON = 1e-05
 LANES = 128
+PIECES = 6
+EARLY = 3
 MESH = pl.DeviceIdType.MESH
 F32 = jnp.float32
 BF16 = jnp.bfloat16
@@ -28,6 +30,37 @@
     return jnp.where(z > -0.5, small * z, jnp.exp(z) - 1.0)
 
 
+def softplus(y):
+    u = jnp.exp(-jnp.abs(y))
+    s = u / (2.0 + u)
+    sq = s * s
+    series = jnp.full_like(s, 1.0 / 17.0)
+    for n in (15.0, 13.0, 11.0, 9.0, 7.0, 5.0, 3.0, 1.0):
+        series = series * sq + 1.0 / n
+    return jnp.maximum(y, 0.0) + 2.0 * s * series
+
+
+def lane_blocks(maps_ref):
+    kinds, heads, size, _ = maps_ref.shape
+    per = LANES // size
+    blocks = []
+    for start in range(0, heads, per):
+        sides = []
+        for kind in range(kinds):
+            if per == 1:
+                sides.append(maps_ref[kind, start])
+                continue
+            tall = []
+            for p in range(per):
+                row = lax.broadcasted_iota(jnp.int32, (size, LANES), 0)
+                col = lax.broadcasted_iota(jnp.int32, (size, LANES), 1)
+                place = jnp.where(col == row + p * size, 1.0, 0.0).astype(BF16)
+                tall.append(dot(maps_ref[kind, start + p], place))
+            sides.append(jnp.concatenate(tall, axis=0).astype(BF16))
+        blocks.append(jnp.concatenate(sides, axis=1))
+    return blocks
+
+
 def silu(v):
     return v * jax.nn.sigmoid(v)
 
@@ -38,10 +71,11 @@
 
 def kernel(
     dims,
-    stream, rec_in, gate_in, taps, gates, rate, extra, n1g, n1b, n2g, n2b, wdense,
+    stream, rec_in, gate_in, taps, small_maps, large_maps, channel_decay, extra, n1g, n1b, n2g, n2b,
+    ids, wts,
     out_w_hbm, rg_hbm, ru_hbm, rd_hbm, sg_hbm, su_hbm, sd_hbm,
     result,
-    padded, halo, carry_own, carry_in, w_own, w_in, out_w, w_gu, w_d, s_gu, s_d,
+    padded, halo, carry_own, carry_in, wdense, w_in, out_w, w_gu, w_d, s_gu, s_d,
     part, part_in, rows, hid, y_part, x_in, z_out, z_in, moe,
     local_sem, halo_sem, carry_send, carry_recv, w_send, w_recv,
     wt_send, wt_recv, tp_send, tp_recv, ag_send, ag_recv, fw_send, fw_recv,
@@ -84,24 +118,30 @@
     )
     halo_copy.start()
 
-    def weight_dst(slot, kind):
-        if kind == 0:
-            return w_gu.at[slot, :, pl.ds(0, fe)]
-        if kind == 1:
-            return w_gu.at[slot, :, pl.ds(fe, fe)]
-        return w_d.at[slot]
-
-    sources = (rg_hbm, ru_hbm, rd_hbm)
+    depth = rg_hbm.shape[0] // 2
+    fe_half = fe // 2
+
+    def weight_src(piece):
+        kind, part_id = piece // 2, piece % 2
+        if kind == 2:
+            return rd_hbm.at[pl.ds(part_id * fe_half, fe_half)]
+        return (rg_hbm, ru_hbm)[kind].at[pl.ds(part_id * depth, depth)]
+
+    def weight_dst(slot, piece):
+        kind, part_id = piece // 2, piece % 2
+        if kind == 2:
+            return w_d.at[slot, pl.ds(part_id * fe_half, fe_half)]
+        return w_gu.at[slot, pl.ds(part_id * depth, depth), pl.ds(kind * fe, fe)]
 
     def weight_out(kind, step):
         return remote(
-            sources[kind], weight_dst(tp, kind),
+            weight_src(kind), weight_dst(tp, kind),
             wt_send.at[kind, step], wt_recv.at[kind, tp],
             (sp, lax.rem(yi + step, pairs) * 2 + half_c),
         )
 
     def weight_mate(kind, slot, step):
-        src = sources[kind] if step == 0 else weight_dst(slot, kind)
+        src = weight_src(kind) if step == 0 else weight_dst(slot, kind)
         return remote(
             src, weight_dst(slot, kind),
             wt_send.at[kind, pairs + step], wt_recv.at[kind, slot], (sp, mate),
@@ -110,18 +150,23 @@
     def pair_slot(step):
         return lax.rem(yi + step, pairs) * 2 + half_c
 
-    for kind in range(3):
+    for piece in range(EARLY):
         for step in range(1, pairs):
-            weight_out(kind, step).start()
+            weight_out(piece, step).start()
     locals_[3].start()
-    for kind in range(3):
-        weight_mate(kind, tp, 0).start()
-        locals_[kind].start()
+    for piece in range(PIECES):
+        weight_mate(piece, tp, 0).start()
+    for i in range(3):
+        locals_[i].start()
     for i in (4, 5, 6):
         locals_[i].start()
 
-    w_own_copy = pltpu.make_async_copy(wdense, w_in.at[sp], local_sem.at[7])
-    w_own_copy.start()
+    expert = lax.broadcasted_iota(jnp.int32, (wdense.shape[0], length), 0)
+    table = jnp.zeros((wdense.shape[0], length), F32)
+    for k in range(ids.shape[0]):
+        table = table + jnp.where(expert == ids[k : k + 1], wts[k : k + 1], 0.0)
+    wdense[...] = table
+    w_in[sp] = table
 
     def w_out(step):
         return remote(
@@ -131,22 +176,31 @@
     @pl.loop(1, sp_n)
     def _(step):
         w_out(step).start()
+
+    small_blocks, large_blocks = lane_blocks(small_maps), lane_blocks(large_maps)
+    rate_rows = -8.0 * softplus(-channel_decay[...])
+    rate = jnp.concatenate([rate_rows[0:1], rate_rows[1:2]], axis=1)
+    tap_rows = [
+        jnp.concatenate([taps[k, 0:1], taps[k, 1:2]], axis=1).astype(F32)
+        for k in range(taps.shape[0])
+    ]
 
     padded[pl.ds(8, length)] = rec_in[...].astype(F32)
     halo_copy.wait()
     border = halo[...].astype(F32)[8:16]
     padded[pl.ds(0, 8)] = jnp.where(sp > 0, border, jnp.zeros_like(border))
     tap_n = taps.shape[0]
-    summed = taps[0:1] * padded[pl.ds(8 - tap_n + 1, length)]
+    summed = tap_rows[0] * padded[pl.ds(8 - tap_n + 1, length)]
     for k in range(1, tap_n):
-        summed = summed + taps[k : k + 1] * padded[pl.ds(8 - tap_n + 1 + k, length)]
+        summed = summed + tap_rows[k] * padded[pl.ds(8 - tap_n + 1 + k, length)]
     conv = summed.astype(BF16)
-    half = chans // 2
-    first = dot(conv[:, :half], gates[0])
-    second = dot(conv[:, half:], gates[1])
-    recur = jax.nn.sigmoid(jnp.concatenate([first[:, :half], second[:, :half]], axis=1))
-    inp = jax.nn.sigmoid(jnp.concatenate([first[:, half:], second[:, half:]], axis=1))
-    log_decay = recur * rate[...] + extra[...]
+    outs = [
+        dot(conv[:, i * LANES : (i + 1) * LANES], maps)
+        for i, maps in enumerate(small_blocks + large_blocks)
+    ]
+    recur = jax.nn.sigmoid(jnp.concatenate([o[:, :LANES] for o in outs], axis=1))
+    inp = jax.nn.sigmoid(jnp.concatenate([o[:, LANES:] for o in outs], axis=1))
+    log_decay = recur * rate + extra[...]
     decay = jnp.exp(log_decay)
     state = jnp.sqrt(-expm1_negative(2.0 * log_decay)) * inp * conv.astype(F32)
     row_id = lax.broadcasted_iota(jnp.int32, (length, chans), 0)
@@ -206,6 +260,9 @@
 
     for step in range(1, tp_n):
         part_out(step).start()
+    for piece in range(EARLY, PIECES):
+        for step in range(1, pairs):
+            weight_out(piece, step).start()
     mixed = part[tp].astype(F32)
     for step in range(1, tp_n):
         who = lax.rem(tp + step, tp_n)
@@ -242,6 +299,14 @@
             wt_send.at[kind, 0], wt_recv.at[kind, slot], (sp, mate),
         )
 
+    def relay(piece):
+        for step in range(1, pairs):
+            weight_arrival(piece, pair_slot(step)).wait_recv()
+            weight_mate(piece, pair_slot(step), step).start()
+
+    for piece in range(EARLY):
+        relay(piece)
+
     locals_[4].wait()
     locals_[5].wait()
     locals_[6].wait()
@@ -254,18 +319,39 @@
         who = lax.rem(sp + step, sp_n)
         remote(wdense, w_in.at[who], w_send.at[0], w_recv.at[who], (sp, tp)).wait_recv()
 
-    w_own_copy.wait()
-    for kind in range(3):
-        for step in range(1, pairs):
-            weight_arrival(kind, pair_slot(step)).wait_recv()
-            weight_mate(kind, pair_slot(step), step).start()
-    for kind in range(3):
-        locals_[kind].wait()
+    for i in range(3):
+        locals_[i].wait()
+
+    @pl.loop(1, outer)
+    def _(step):
+        mine = lax.rem(zi + step, outer) * inner + xi
+        ag_arrival(mine).wait_recv()
+        forward(mine).start()
+
+    for piece in range(EARLY, PIECES):
+        relay(piece)
+
+    @pl.loop(0, outer)
+    def _(step):
+        ag_arrival(step * inner + other_x).wait_recv()
+
+    for piece in range(PIECES):
         for step in range(pairs):
-            weight_arrival(kind, lax.rem(yi + step, pairs) * 2 + 1 - half_c).wait_recv()
+            weight_arrival(piece, lax.rem(yi + step, pairs) * 2 + 1 - half_c).wait_recv()
 
     width = stream.shape[1]
     grp = inner * quarter
+    batch = min(sp_n, 8)
+
+    @pl.loop(0, sp_n // batch)
+    def _(i):
+        block = rows[pl.ds(i * batch, batch)].reshape(batch * quarter, width)
+        for t in range(tp_n):
+            gu = dot(block, w_gu[t])
+            act = (silu(gu[:, :fe]) * gu[:, fe:]).astype(BF16)
+            hid[pl.ds(i * batch, batch), :, t * fe : (t + 1) * fe] = act.reshape(
+                batch, quarter, fe
+            )
 
     def x_out(zj):
         return remote(
@@ -273,26 +359,20 @@
             (x_peer, tp),
         )
 
-    @pl.loop(0, outer)
+    own_rows = lax.broadcasted_iota(jnp.int32, (quarter, length), 0) + tp * quarter
+    pick = lax.broadcasted_iota(jnp.int32, (quarter, length), 1) == own_rows
+
+    @pl.loop(1, outer + 1)
     def _(step):
         zj = lax.rem(zi + step, outer)
-        mine, theirs = zj * inner + xi, zj * inner + other_x
-
-        @pl.when(step > 0)
-        def _():
-            ag_arrival(mine).wait_recv()
-            forward(mine).start()
-
-        ag_arrival(theirs).wait_recv()
-        block = rows[pl.ds(zj * inner, inner)].reshape(grp, width)
-        for t in range(tp_n):
-            gu = dot(block, w_gu[t])
-            hid[:, t * fe : (t + 1) * fe] = (silu(gu[:, :fe]) * gu[:, fe:]).astype(BF16)
-        wv = w_in[pl.ds(zj * inner, inner)].reshape(grp, w_in.shape[2])
-        lane = lax.broadcasted_iota(jnp.int32, wv.shape, 1)
-        weight = jnp.sum(jnp.where(lane == sp, wv, 0.0), axis=1, keepdims=True)
-        value = weight * dot(hid[...], w_d[...].reshape(tp_n * fe, width))
-        y_part[pl.ds(zj * inner, inner)] = value.astype(BF16).reshape(inner, quarter, width)
+        block = hid[pl.ds(zj * inner, inner)].reshape(grp, tp_n * fe)
+        value = dot(block, w_d[...].reshape(tp_n * fe, width))
+        for j in range(inner):
+            line = w_in[zj * inner + j, pl.ds(sp, 1)]
+            weight = jnp.sum(jnp.where(pick, line, 0.0), axis=1, keepdims=True)
+            y_part[zj * inner + j] = (
+                weight * value[j * quarter : (j + 1) * quarter]
+            ).astype(BF16)
         x_out(zj).start()
 
     def z_send(step):
@@ -320,7 +400,7 @@
 
     result[...] = layer_norm(moe[...], n2g[...], n2b[...]).astype(BF16)
 
-    for kind in range(3):
+    for kind in range(PIECES):
         for step in range(1, pairs):
             weight_out(kind, step).wait_send()
             weight_mate(kind, pair_slot(step), step).wait_send()
@@ -342,14 +422,6 @@
     def _(step):
         forward(step * inner + xi).wait_send()
         x_out(step).wait_send()
-
-
-def block_diagonal(maps):
-    kinds, heads, size, _ = maps.shape
-    eye = jnp.eye(heads, dtype=maps.dtype)
-    spread = maps[:, :, :, None, :] * eye[None, :, None, :, None]
-    spread = spread.reshape(kinds, heads * size, heads * size)
-    return jnp.concatenate([spread[i] for i in range(kinds)], axis=1)
 
 
 def shards(
@@ -383,15 +455,7 @@
     quarter, width = stream.shape
     fe = routed_gate_weight.shape[2]
     fs = shared_gate_weight.shape[1]
-    lanes = -(-sp_n // LANES) * LANES
     flat = lambda a: a.reshape(a.shape[0], chans)
-    gates = jnp.stack([block_diagonal(first_group_gates), block_diagonal(second_group_gates)])
-    rate = (-8.0 * jax.nn.softplus(-channel_decay)).reshape(1, chans)
-    own = lax.axis_index("tp") * quarter
-    ids = lax.dynamic_slice_in_dim(routed_expert_index, own, quarter, 0)
-    wts = lax.dynamic_slice_in_dim(routed_expert_weight, own, quarter, 0)
-    hits = ids[:, :, None] == jnp.arange(lanes, dtype=jnp.int32)[None, None, :]
-    wdense = jnp.sum(jnp.where(hits, wts[:, :, None], 0.0), axis=1)
     vec = lambda a: a.reshape(1, width)
     vmem = pl.BlockSpec(memory_space=pltpu.VMEM)
     hbm = pl.BlockSpec(memory_space=pl.ANY)
@@ -401,15 +465,15 @@
     return pl.pallas_call(
         functools.partial(kernel, dims),
         out_shape=jax.ShapeDtypeStruct(block, BF16),
-        in_specs=[vmem] * 12 + [hbm] * 7,
+        in_specs=[vmem] * 14 + [hbm] * 7,
         out_specs=vmem,
         scratch_shapes=[
             pltpu.VMEM((length + 8, chans), F32),
             pltpu.VMEM((16, chans), BF16),
             pltpu.VMEM((8, chans), F32),
             pltpu.VMEM((sp_n, 8, chans), F32),
-            pltpu.VMEM((8, LANES), F32),
-            pltpu.VMEM((sp_n, quarter, lanes), F32),
+            pltpu.VMEM((sp_n, length), F32),
+            pltpu.VMEM((sp_n, sp_n, length), F32),
             pltpu.VMEM((chans, width), BF16),
             pltpu.VMEM((tp_n, width, 2 * fe), BF16),
             pltpu.VMEM((tp_n, fe, width), BF16),
@@ -418,7 +482,7 @@
             pltpu.VMEM((tp_n,) + block, BF16),
             pltpu.VMEM((tp_n,) + block, BF16),
             pltpu.VMEM((sp_n,) + block, BF16),
-            pltpu.VMEM((inner * quarter, tp_n * fe), BF16),
+            pltpu.VMEM((sp_n, quarter, tp_n * fe), BF16),
             pltpu.VMEM((sp_n,) + block, BF16),
             pltpu.VMEM((outer,) + block, BF16),
             pltpu.VMEM((outer,) + block, BF16),
@@ -430,8 +494,8 @@
             dma((sp_n,)),
             dma((sp_n,)),
             dma((sp_n,)),
-            dma((3, 2 * pairs)),
-            dma((3, tp_n)),
+            dma((PIECES, 2 * pairs)),
+            dma((PIECES, tp_n)),
             dma((tp_n,)),
             dma((tp_n,)),
             dma((outer,)),
@@ -450,15 +514,17 @@
         stream,
         flat(recurrence_input),
         flat(output_gate_input),
-        flat(convolution_taps).astype(F32),
-        gates,
-        rate,
+        convolution_taps,
+        first_group_gates,
+        second_group_gates,
+        channel_decay,
         flat(position_log_extra),
         vec(first_norm_gain),
         vec(first_norm_bias),
         vec(second_norm_gain),
         vec(second_norm_bias),
-        wdense,
+        routed_expert_index.T,
+        routed_expert_weight.T,
         recurrence_output_weight.reshape(chans, width),
         routed_gate_weight.reshape(width, fe),
         routed_up_weight.reshape(width, fe),

time: 108 us -> 83.7 us (0.78)
  Pallas kernels: 97.6 us -> 77.1 us
  other arithmetic: 3.13 us -> 0 us
    pallas_call x1, Pallas kernels: 97.6 us -> 77.1 us  [shards(): pl.pallas_call(functools.partial(kernel, dims), out_shape=jax.ShapeDtypeS...]
    mul x2 -> x0, other arithmetic: 1.52 us -> none  [block_diagonal(): spread = maps[:, :, :, None, :] * eye[None, :, None, :, None]]
    unnamed x20 -> x4, local copies, waits for them, and re-layouts: 5.52 us -> 6.38 us
where the time goes in v2:
time: 83.7 us; the launch traced here: 83.5 us
  Pallas kernels  77.1 us (92%)
  local copies, waits for them, and re-layouts  6.38 us (8%)
    pallas_call x1, Pallas kernels, shards(): pl.pallas_call(functools.partial(kernel, dims), out_shape=jax.ShapeDtypeS...  77.1 us
    unnamed x4, local copies, waits for them, and re-layouts  6.38 us

profile of v2, /device:TPU:0, one launch (start us, length us, event | category | flops | bytes accessed | tf_op | source)
XLA Modules:
  0.0 83.5 jit_solution(12635204757703253968)
XLA Ops:
  0.0 1.6 %copy.22 = bf16[16,8,2,256]{3,1,2,0:T(8,128)(2,1)} copy(bf16[16,8,2,256]{3,2,1,0:T(2,128)(2,1)} %bitcast.24) | data formatting | bytes 262144
  1.6 1.6 %copy.23 = bf16[16,8,2,256]{3,1,2,0:T(8,128)(2,1)} copy(bf16[16,8,2,256]{3,2,1,0:T(2,128)(2,1)} %bitcast.25) | data formatting | bytes 262144
  3.2 1.7 %copy.24 = f32[16,8,2,256]{3,1,2,0:T(8,128)} copy(f32[16,8,2,256]{3,2,1,0:T(2,128)} %bitcast.23) | data formatting | bytes 524288
  4.8 77.1 %shard_map.199 = bf16[32,2048]{1,0:T(8,128)(2,1)} custom-call(bf16[32,2048]{1,0:T(8,128)(2,1)} %stream.1, bf16[128,512]{1,0:T(8,128)(2,1)} %bitcast.21, bf16[128,512]{1,0:T(8,128)(2,1)} %bitcast.22, bf16[4,2,256]{2,1,0:T(2,128)(2,1)} %taps.1, bf16[2,4,64,64]{3,2,1,0:T(8,128)(2,1)} %small_maps.1, bf16[2,2,128,128]{3,2,1,0:T(8,128)(2,1)} %large_maps.1, ...), custom_call_target="tpu_custom_call" | custom-call | tf_op jit(solution)/shard_map/pallas_call | solution.py:465
  81.9 1.6 %copy.26 = bf16[32,2048]{1,0:T(8,128)(2,1)} copy(bf16[32,2048]{1,0:T(8,128)(2,1)} %shard_map.199) | data formatting | bytes 262144
